TPU v7x, 32 devices: a whole 2x2x4 slice. The times are simulated.
32 devices in a mesh: grp: 2 (over y), sp: 4 (over z), tp: 4 (over x, core).
Axes of the slice: x: 2, y: 2, z: 4, core: 2. Of those that a mesh axis runs over, the one named last changes fastest.
Arguments:
- tokens: bfloat16 [1280, 2048], P(('grp', 'sp')), parts along dimension 0, may hold values from -6 to 6
- norm_gain: float32 [2048], replicated, may hold values from 0.6 to 5
- query_weight: bfloat16 [2048, 2048], P('sp', 'tp')
- key_weight: bfloat16 [2048, 512], P('sp', 'tp')
- value_weight: bfloat16 [2048, 512], P('sp', 'tp'), may hold values from -0.125 to 0.125
- map_lambda: float32 [16], P('tp'), may hold values from 0.3 to 0.8
- head_gain: float32 [16, 128], P('tp'), may hold values from 0.1 to 1.9
- attn_out_weight: bfloat16 [2048, 2048], P('tp', 'sp'), may hold values from -0.125 to 0.125
- pool_out_weight: bfloat16 [2048, 2048], P('tp', 'sp'), may hold values from -0.09375 to 0.09375
Outputs:
- mixed_rows: bfloat16 [1280, 2048], P(('grp', 'sp', 'tp')), parts along dimension 0
- log_totals: float32 [2, 16, 1280], P(None, 'tp', ('grp', 'sp')), parts along dimension 2
There are 2 independent parts, one for each index of `grp`. A program takes and returns all parts, laid end to end along the dimension named above; an argument that names none is the same for every part. Nothing has to cross between parts.
All inputs are finite; a program needn't handle non-finite values.
Results may differ from a plain program's by a relative error of at most 0.013.
The roundings to bfloat16 on the way count: a program that leaves them out, or rounds other values in their place, can miss the bound.
Values may be sent and summed in bfloat16 or wider, within the bound.
A program may use at most 64 MiB of HBM per device.

v0:
```python
import math
import jax
import jax.numpy as jnp
from jax import lax
from jax.sharding import PartitionSpec as P

HD = 64
VD = 128
POOL_SPAN = 16
epsilon = 1e-06
very_low = -1e30


def extended(cells, sides, width):
    for axis, dim in sides:
        count = lax.axis_size(axis)
        ends = count - 1
        head = lax.slice_in_dim(cells, 0, width, axis=dim)
        tail = lax.slice_in_dim(cells, cells.shape[dim] - width, cells.shape[dim], axis=dim)
        cells = jnp.concatenate(
            [
                lax.ppermute(tail, axis, [(i, (i + 1) % count) for i in range(ends)]),
                cells,
                lax.ppermute(head, axis, [((i + 1) % count, i) for i in range(ends)]),
            ],
            axis=dim,
        )
    return cells


def add_products(totals, pieces, source):
    results = []
    for running, piece in zip(totals, pieces):
        results.append(jnp.dot(source, piece, preferred_element_type=jnp.float32))
    return tuple(results)


def on_device(
    tokens,
    norm_gain,
    query_weight,
    key_weight,
    value_weight,
    map_lambda,
    head_gain,
    attn_out_weight,
    pool_out_weight,
):
    tokens_wide = tokens.astype(jnp.float32)
    normed = (
        tokens_wide
        * lax.rsqrt(jnp.mean(tokens_wide * tokens_wide, axis=-1, keepdims=True) + epsilon)
        * norm_gain
    ).astype(jnp.bfloat16)
    row_count = normed.shape[0]
    sp_index = lax.axis_index("sp")
    tp_index = lax.axis_index("tp")
    group_width = pool_out_weight.shape[0]
    local_heads = map_lambda.shape[0]
    key_heads = value_weight.shape[1] // VD
    group_heads = local_heads // key_heads
    q_empty = jnp.zeros((row_count, query_weight.shape[1]), jnp.float32)
    k_empty = jnp.zeros((row_count, key_weight.shape[1]), jnp.float32)
    v_empty = jnp.zeros((row_count, value_weight.shape[1]), jnp.float32)
    q_acc, k_acc, v_acc = add_products(
        (q_empty, k_empty, v_empty),
        (
            lax.all_gather(query_weight, "sp", axis=0, tiled=True),
            lax.all_gather(key_weight, "sp", axis=0, tiled=True),
            lax.all_gather(value_weight, "sp", axis=0, tiled=True),
        ),
        normed,
    )
    queries = q_acc.astype(jnp.bfloat16).reshape(row_count, key_heads, group_heads, 2, HD)
    keys_flat = k_acc.astype(jnp.bfloat16)
    values_flat = v_acc.astype(jnp.bfloat16)

    def key_block(state_now, key_pair):
        maxima, totals, accums = state_now
        key_blk, val_blk = key_pair
        scores = jnp.einsum(
            "qhgmd,khmd->hgmqk", queries, key_blk, preferred_element_type=jnp.float32
        ) * HD ** (-0.5)
        highest = jnp.maximum(maxima, jnp.max(scores, axis=-1))
        factor = jnp.exp(maxima - highest)
        weights = jnp.exp(scores - highest[..., None])
        totals = totals * factor + jnp.sum(weights, axis=-1)
        accums = accums * factor[..., None] + jnp.einsum(
            "hgmqk,khe->hgmqe",
            weights.astype(jnp.bfloat16),
            val_blk,
            preferred_element_type=jnp.float32,
        )
        return ((highest, totals, accums), None)

    start_state = (
        jnp.full((key_heads, group_heads, 2, row_count), very_low, jnp.float32),
        jnp.zeros((key_heads, group_heads, 2, row_count), jnp.float32),
        jnp.zeros((key_heads, group_heads, 2, row_count, VD), jnp.float32),
    )
    key_piece = lax.all_gather(keys_flat, "sp", axis=0, tiled=True)
    val_piece = lax.all_gather(values_flat, "sp", axis=0, tiled=True)
    piece_len = key_piece.shape[0]
    block_len = math.gcd(piece_len, 512)
    key_blocks = key_piece.reshape(piece_len // block_len, block_len, key_heads, 2, HD)
    val_blocks = val_piece.reshape(piece_len // block_len, block_len, key_heads, VD)
    state_next, unused = lax.scan(key_block, start_state, (key_blocks, val_blocks))
    maxima, totals, accums = state_next
    log_parts = maxima + jnp.log(totals)
    log_totals = jnp.transpose(log_parts, (2, 0, 1, 3)).reshape(2, local_heads, row_count)
    reads = accums / totals[..., None]
    contrast = reads[:, :, 0] - map_lambda.reshape(key_heads, group_heads, 1, 1) * reads[:, :, 1]
    scaled = (
        contrast
        * lax.rsqrt(jnp.mean(contrast * contrast, axis=-1, keepdims=True) + epsilon)
        * head_gain.reshape(key_heads, group_heads, 1, VD)
    )
    attention_head_rows = (
        jnp.transpose(scaled, (2, 0, 1, 3))
        .reshape(row_count, local_heads * VD)
        .astype(jnp.bfloat16)
    )
    head_rows, log_totals = (attention_head_rows, log_totals)
    own_chan = lax.dynamic_slice_in_dim(normed, tp_index * group_width, group_width, 1)
    reach = POOL_SPAN // 2
    padded = extended(own_chan, (("sp", 0),), reach)
    window = jnp.left_shift(jnp.int32(2), tp_index)
    half_span = window // 2
    running = jnp.zeros((row_count, group_width), jnp.float32)
    for offset in range(POOL_SPAN):
        piece = lax.dynamic_slice_in_dim(padded, reach - half_span + offset, row_count, 0).astype(
            jnp.float32
        )
        running = running + jnp.where(offset < window, piece, 0.0)
    seq_len = row_count * lax.axis_size("sp")
    position = sp_index * row_count + jnp.arange(row_count, dtype=jnp.int32)
    lower_edge = jnp.clip(position - half_span, 0, seq_len)
    upper_edge = jnp.clip(position + window - half_span, 0, seq_len)
    counts_f = (upper_edge - lower_edge).astype(jnp.float32)[:, None]
    pooled = (running / counts_f - own_chan.astype(jnp.float32)).astype(jnp.bfloat16)
    attn_whole, pool_whole = (
        lax.all_gather(attn_out_weight, "sp", axis=1, tiled=True),
        lax.all_gather(pool_out_weight, "sp", axis=1, tiled=True),
    )
    mixed = lax.psum_scatter(
        (
            jnp.dot(head_rows, attn_whole, preferred_element_type=jnp.float32)
            + jnp.dot(pooled, pool_whole, preferred_element_type=jnp.float32)
        ).astype(jnp.bfloat16),
        "tp",
        scatter_dimension=0,
        tiled=True,
    )
    return (mixed, log_totals)


def solution(mesh):
    placed = (
        P(("grp", "sp"), None),
        P(),
        P("sp", "tp"),
        P("sp", "tp"),
        P("sp", "tp"),
        P("tp"),
        P("tp", None),
        P("tp", "sp"),
        P("tp", "sp"),
    )
    return jax.shard_map(
        on_device,
        mesh=mesh,
        in_specs=placed,
        out_specs=(P(("grp", "sp", "tp"), None), P(None, "tp", ("grp", "sp"))),
        check_vma=False,
    )
```

profile of v0, /device:TPU:0, one launch (start us, length us, event | category | flops | bytes accessed | tf_op | source)
XLA Modules:
  0.0 200.9 jit_solution(6198464641306412881)
XLA Ops:
  7.2 0.7 all-gather.4.cloned.1.call-update
  8.0 0.7 all-gather.6.cloned.1.call-update
  8.7 1.3 fusion.15
  10.0 1.0 fusion.17
  11.0 5.0 %collective-permute-start = (bf16[8,512]{1,0:T(8,128)(2,1)S(1)}, bf16[8,512]{1,0:T(8,128)(2,1)S(1)}, u32[]{:S(2)}, u32[]{:S(2)}) collective-permute-start(bf16[8,512]{1,0:T(8,128)(2,1)S(1)} %get-tuple-element.102), channel_id=1, source_target_pairs={{0,4},{4,8},{8,12},{1,5},{5,9},{9,13},{2,6},{6,10},{10,14},{3,7},{... | collective-permute-start | bytes 24584 | tf_op jit(solution)/shard_map/ppermute | solution.py:22
  16.0 1.3 collective-permute-start.1
  17.4 24.1 %all_gather.21 = bf16[2048,128]{1,0:T(8,128)(2,1)S(1)} all-gather(bf16[512,128]{1,0:T(8,128)(2,1)S(1)} %copy-done.1), channel_id=1, replica_groups=mesh['grp'=2,'sp'=4,'tp'=4] {'sp'}, dimensions={0}, use_global_device_ids=true | all-gather | bytes 655360 | tf_op jit(solution)/shard_map/all_gather | solution.py:69
  41.9 15.2 %all_gather.22 = bf16[640,128]{1,0:T(8,128)(2,1)S(1)} all-gather(bf16[160,128]{1,0:T(8,128)(2,1)S(1)} %convolution_convert_fusion.2), channel_id=1, replica_groups=mesh['grp'=2,'sp'=4,'tp'=4] {'sp'}, dimensions={0}, use_global_device_ids=true | all-gather | bytes 204800 | tf_op jit(solution)/shard_map/all_gather | solution.py:101
  57.1 21.5 %all_gather.24 = bf16[2048,128]{1,0:T(8,128)(2,1)S(1)} all-gather(bf16[512,128]{1,0:T(8,128)(2,1)S(1)} %copy-done.2), channel_id=1, replica_groups=mesh['grp'=2,'sp'=4,'tp'=4] {'sp'}, dimensions={0}, use_global_device_ids=true | all-gather | bytes 655360 | tf_op jit(solution)/shard_map/all_gather | solution.py:70
  78.9 14.8 %all_gather.25 = bf16[640,128]{1,0:T(8,128)(2,1)S(1)} all-gather(bf16[160,128]{1,0:T(8,128)(2,1)S(1)} %convolution_convert_fusion.1), channel_id=1, replica_groups=mesh['grp'=2,'sp'=4,'tp'=4] {'sp'}, dimensions={0}, use_global_device_ids=true | all-gather | bytes 204800 | tf_op jit(solution)/shard_map/all_gather | solution.py:102
  94.2 2.1 %convolution_convert_fusion = bf16[160,512]{1,0:T(8,128)(2,1)S(1)} fusion(bf16[160,2048]{1,0:T(8,128)(2,1)S(1)} %fusion.17, bf16[2048,512]{1,0:T(8,128)(2,1)} %all-gather.4.cloned.1.call-done), kind=kOutput, calls=%fused_computation.29 | convolution fusion | flops 335626240 | bytes 2916352 | tf_op jit(solution)/shard_map/dot_general | solution.py:34
  96.6 8.5 %while.15 = (s32[]{:T(128)}, f32[1,4,2,160]{3,1,2,0:T(4,128)S(1)}, f32[1,4,2,160]{3,1,2,0:T(4,128)S(1)}, f32[1,4,2,160,128]{4,3,2,1,0:T(8,128)S(1)}, bf16[5,128,...) while((s32[]{:T(128)}, f32[1,4,2,160]{3,1,2,0:T(4,128)S(1)}, ...), condition=%wide.region_4.5_spmd.clone, body=%wide.region_1.4_spmd.clone.sunk | while | flops 64232960 | bytes 3694705 | solution.py:107
  96.6 0.6 fusion.78
  97.2 0.6 fusion.80
  98.3 0.6 fusion.78
  100.0 0.6 fusion.78
  101.7 0.6 fusion.78
  103.4 0.6 fusion.78
  105.9 16.4 %all-gather.6.cloned.1.call-done = bf16[512,2048]{1,0:T(8,128)(2,1)} async-done(((bf16[512,512]{1,0:T(8,128)(2,1)}), bf16[512,2048]{1,0:T(8,128)(2,1)}) %all-gather.6.cloned.1.call-update) | async-done | bytes 2097168 | tf_op jit(solution)/shard_map/all_gather | solution.py:142
  122.4 2.1 %fusion.21 = f32[160,2048]{1,0:T(8,128)S(1)} fusion(bf16[512,2048]{1,0:T(8,128)(2,1)} %all-gather.6.cloned.1.call-done, bf16[20,8,4,128]{3,2,1,0:T(4,128)(2,1)S(1)} %bitcast.102), kind=kOutput, calls=%fused_computation.42 | convolution fusion | flops 335544320 | bytes 3571712 | tf_op jit(solution)/shard_map/dot_general | solution.py:147
  124.5 44.1 %all-gather.8.cloned.1.call-done = bf16[512,2048]{1,0:T(8,128)(2,1)} async-done(((bf16[512,512]{1,0:T(8,128)(2,1)}), bf16[512,2048]{1,0:T(8,128)(2,1)}) %all-gather.8.cloned.1.call-update) | async-done | bytes 2097168 | tf_op jit(solution)/shard_map/all_gather | solution.py:143
  168.6 4.3 %fusion.14 = bf16[160,2048]{1,0:T(8,128)(2,1)} fusion(f32[160,2048]{1,0:T(8,128)S(1)} %fusion.21, bf16[512,2048]{1,0:T(8,128)(2,1)} %all-gather.8.cloned.1.call-done, bf16[160,512]{1,0:T(8,128)(2,1)S(1)} %constant_dynamic-slice_fusion.1, f32[160]{0:T(256)S(1)} %subtract_convert_fusion.2, bf16[176,512]{1,0:T(8,128)(2,1)S(1)} %pad_maximum_fusion, ...), kind=kOutput, calls=%fused_computation.23 | convolution fusion | flops 340377600 | bytes 6849616 | tf_op jit(solution)/shard_map/dot_general | solution.py:148
  172.9 0.6 add_bitcast_fusion
  173.5 20.8 %reduce-scatter.2.cloned.1.call-done = bf16[40,2048]{1,0:T(8,128)(2,1)} async-done(((bf16[160,2048]{1,0:T(8,128)(2,1)}), bf16[40,2048]{1,0:T(8,128)(2,1)}) %reduce-scatter.2.cloned.1.call-update) | async-done | bytes 163856 | tf_op jit(solution)/shard_map/reduce_scatter | solution.py:145
  (68 shorter events, 6.7 us)
Async XLA Ops:
  7.2 2.9 %copy-start = (bf16[160,2048]{1,0:T(8,128)(2,1)S(1)}, bf16[160,2048]{1,0:T(8,128)(2,1)}, u32[]{:S(2)}) copy-start(bf16[160,2048]{1,0:T(8,128)(2,1)} %param.11) | copy-start | bytes 1966084
  7.2 10.3 %copy-start.1 = (bf16[512,128]{1,0:T(8,128)(2,1)S(1)}, bf16[512,128]{1,0:T(8,128)(2,1)}, u32[]{:S(2)}) copy-start(bf16[512,128]{1,0:T(8,128)(2,1)} %param.14) | copy-start | bytes 393220
  7.2 87.0 %all-gather.4.cloned.1.call-start = ((), (), s32[]{:S(2)}) async-start(), calls=%async_computation.1 | async-start | bytes 2621440 | tf_op jit(solution)/shard_map/all_gather | solution.py:68
  7.9 114.4 %all-gather.6.cloned.1.call-start = ((), (), s32[]{:S(2)}) async-start(), calls=%async_computation.2 | async-start | bytes 2621440 | tf_op jit(solution)/shard_map/all_gather | solution.py:142
  8.7 159.9 %all-gather.8.cloned.1.call-start = ((), (), s32[]{:S(2)}) async-start(), calls=%async_computation.3 | async-start | bytes 2621440 | tf_op jit(solution)/shard_map/all_gather | solution.py:143
  10.0 47.0 %copy-start.2 = (bf16[512,128]{1,0:T(8,128)(2,1)S(1)}, bf16[512,128]{1,0:T(8,128)(2,1)}, u32[]{:S(2)}) copy-start(bf16[512,128]{1,0:T(8,128)(2,1)} %param.15) | copy-start | bytes 393220
  11.0 83.1 %collective-permute-start = (bf16[8,512]{1,0:T(8,128)(2,1)S(1)}, bf16[8,512]{1,0:T(8,128)(2,1)S(1)}, u32[]{:S(2)}, u32[]{:S(2)}) collective-permute-start(bf16[8,512]{1,0:T(8,128)(2,1)S(1)} %get-tuple-element.102), channel_id=1, source_target_pairs={{0,4},{4,8},{8,12},{1,5},{5,9},{9,13},{2,6},{6,10},{10,14},{3,7},{... | collective-permute-start | bytes 24584 | tf_op jit(solution)/shard_map/ppermute | solution.py:22
  16.0 78.2 %collective-permute-start.1 = (bf16[8,512]{1,0:T(8,128)(2,1)S(1)}, bf16[8,512]{1,0:T(8,128)(2,1)S(1)}, u32[]{:S(2)}, u32[]{:S(2)}) collective-permute-start(bf16[8,512]{1,0:T(8,128)(2,1)S(1)} %get-tuple-element.103), channel_id=1, source_target_pairs={{4,0},{8,4},{12,8},{5,1},{9,5},{13,9},{6,2},{10,6},{14,10},{7,3},{... | collective-permute-start | bytes 24584 | tf_op jit(solution)/shard_map/ppermute | solution.py:24
  17.3 177.0 %reduce-scatter.2.cloned.1.call-start = ((), (), s32[]{:S(2)}) async-start(), calls=%async_computation.4 | async-start | bytes 819200 | tf_op jit(solution)/shard_map/reduce_scatter | solution.py:145
  96.5 8.8 %copy-start.4 = (f32[4]{0:T(128)S(1)}, f32[4]{0:T(128)}, u32[]{:S(2)}) copy-start(f32[4]{0:T(128)} %param.16) | copy-start | bytes 52
  96.5 9.1 %copy-start.3 = (f32[4,128]{1,0:T(4,128)S(1)}, f32[4,128]{1,0:T(4,128)}, u32[]{:S(2)}) copy-start(f32[4,128]{1,0:T(4,128)} %param.17) | copy-start | bytes 6148
Sparse Core Ops, SparseCore 0:
  9.6 66.0 all-gather.3
  77.3 45.0 all-gather.5
  123.9 44.6 all-gather.7
  173.1 21.2 reduce-scatter.1
where the time goes:
time: 201 us
  waiting for transfers between devices  82.8 us (41%)
  blocking collectives  75.5 us (38%)
  matrix products  14.4 us (7%)
  between operations  14.2 us (7%)
  other arithmetic  6.68 us (3%)
  starting transfers between devices  6.4 us (3%)
    all_gather x1, waiting for transfers between devices, on_device(): lax.all_gather(pool_out_weight, 'sp', axis=1, tiled=True)  44.1 us
    all_gather x1, blocking collectives, on_device(): lax.all_gather(key_weight, 'sp', axis=0, tiled=True)  24.1 us
    all_gather x1, blocking collectives, on_device(): lax.all_gather(value_weight, 'sp', axis=0, tiled=True)  21.5 us
    reduce_scatter x1, waiting for transfers between devices, on_device(): lax.psum_scatter((jnp.dot(head_rows, attn_whole, preferred_element_type=j...  20.8 us
    all_gather x1, waiting for transfers between devices, on_device(): lax.all_gather(attn_out_weight, 'sp', axis=1, tiled=True)  16.4 us
    all_gather x1, blocking collectives, on_device(): key_piece = lax.all_gather(keys_flat, 'sp', axis=0, tiled=True)  15.2 us
    all_gather x1, blocking collectives, on_device(): val_piece = lax.all_gather(values_flat, 'sp', axis=0, tiled=True)  14.8 us
    ppermute x1, starting transfers between devices, extended(): lax.ppermute(tail, axis, [(i, (i + 1) % count) for i in range(ends)])  4.96 us
  transfers between devices with their start and end apart: 6, of which 3 were waited for; matrix products, arithmetic and copies ran while one was open for 9% of the time, Pallas kernels for 0%

commit v1 on v0

--- a/solution.py
+++ b/solution.py
@@ -98,7 +98,12 @@
         jnp.zeros((key_heads, group_heads, 2, row_count), jnp.float32),
         jnp.zeros((key_heads, group_heads, 2, row_count, VD), jnp.float32),
     )
-    key_piece = lax.all_gather(keys_flat, "sp", axis=0, tiled=True)
+    ring = [keys_flat]
+    for hop in range(3):
+        ring.append(lax.ppermute(ring[-1], "sp", [(dev, (dev + 1) % 4) for dev in range(4)]))
+    key_piece = jnp.roll(
+        jnp.concatenate(ring[::-1], axis=0), (lax.axis_index("sp") + 1) * ring[0].shape[0], axis=0
+    )
     val_piece = lax.all_gather(values_flat, "sp", axis=0, tiled=True)
     piece_len = key_piece.shape[0]
     block_len = math.gcd(piece_len, 512)

time: 201 us -> 199 us (0.990)
  blocking collectives: 75.5 us -> 61 us
  waiting for transfers between devices: 82.8 us -> 95.2 us
    all_gather x1 -> x0, blocking collectives: 15.2 us -> none  [on_device(): key_piece = lax.all_gather(keys_flat, 'sp', axis=0, tiled=True)]
    all_gather x1, waiting for transfers between devices: 16.4 us -> 24.1 us  [on_device(): lax.all_gather(attn_out_weight, 'sp', axis=1, tiled=True)]
    ppermute x0 -> x3, waiting for transfers between devices: none -> 4.83 us  [on_device(): lax.ppermute(ring[-1], 'sp', [(dev, (dev + 1) % 4) for dev in range(4)])]
    all_gather x1, blocking collectives: 21.5 us -> 24 us  [on_device(): lax.all_gather(value_weight, 'sp', axis=0, tiled=True)]
    ppermute x0 -> x3, starting transfers between devices: none -> 2.54 us  [on_device(): lax.ppermute(ring[-1], 'sp', [(dev, (dev + 1) % 4) for dev in range(4)])]
    ppermute x1, starting transfers between devices: 4.96 us -> 2.65 us  [extended(): lax.ppermute(tail, axis, [(i, (i + 1) % count) for i in range(ends)])]
    all_gather x1, blocking collectives: 24.1 us -> 22 us  [on_device(): lax.all_gather(key_weight, 'sp', axis=0, tiled=True)]
  transfers between devices with their start and end apart: 6 -> 9, of which waited for: 3 -> 4; matrix products, arithmetic and copies ran while one was open for 9% -> 8% of each run, Pallas kernels for 0% -> 0%
where the time goes in v1:
time: 199 us; the launch traced here: 198 us
  waiting for transfers between devices  95.2 us (48%)
  blocking collectives  61 us (31%)
  matrix products  14.3 us (7%)
  between operations  14.1 us (7%)
  starting transfers between devices  6.64 us (3%)
  other arithmetic  5.95 us (3%)
    all_gather x1, waiting for transfers between devices, on_device(): lax.all_gather(pool_out_weight, 'sp', axis=1, tiled=True)  44 us
    all_gather x1, waiting for transfers between devices, on_device(): lax.all_gather(attn_out_weight, 'sp', axis=1, tiled=True)  24.1 us
    all_gather x1, blocking collectives, on_device(): lax.all_gather(value_weight, 'sp', axis=0, tiled=True)  24 us
    all_gather x1, blocking collectives, on_device(): lax.all_gather(key_weight, 'sp', axis=0, tiled=True)  22 us
    reduce_scatter x1, waiting for transfers between devices, on_device(): lax.psum_scatter((jnp.dot(head_rows, attn_whole, preferred_element_type=j...  20.8 us
    all_gather x1, blocking collectives, on_device(): val_piece = lax.all_gather(values_flat, 'sp', axis=0, tiled=True)  14.9 us
    ppermute x3, waiting for transfers between devices, on_device(): lax.ppermute(ring[-1], 'sp', [(dev, (dev + 1) % 4) for dev in range(4)])  4.83 us
    dot_general x1, matrix products, on_device(): jnp.dot(pooled, pool_whole, preferred_element_type=jnp.float32)  4.32 us
  transfers between devices with their start and end apart: 9, of which 4 were waited for; matrix products, arithmetic and copies ran while one was open for 8% of the time, Pallas kernels for 0%

profile of v1, /device:TPU:0, one launch (start us, length us, event | category | flops | bytes accessed | tf_op | source)
XLA Modules:
  0.0 198.2 jit_solution(13286622720465916657)
XLA Ops:
  7.2 0.7 all-gather.4.cloned.1.call-update
  8.0 0.7 all-gather.6.cloned.1.call-update
  8.7 1.3 fusion.15
  10.0 22.0 %all_gather.18 = bf16[2048,128]{1,0:T(8,128)(2,1)S(1)} all-gather(bf16[512,128]{1,0:T(8,128)(2,1)} %param.14), channel_id=1, replica_groups=mesh['grp'=2,'sp'=4,'tp'=4] {'sp'}, dimensions={0}, use_global_device_ids=true | all-gather | bytes 655360 | tf_op jit(solution)/shard_map/all_gather | solution.py:69
  32.6 0.9 collective-permute-start
  33.6 2.7 %collective-permute-start.3 = (bf16[8,512]{1,0:T(8,128)(2,1)S(1)}, bf16[8,512]{1,0:T(8,128)(2,1)S(1)}, u32[]{:S(2)}, u32[]{:S(2)}) collective-permute-start(bf16[8,512]{1,0:T(8,128)(2,1)S(1)} %get-tuple-element.102), channel_id=1, source_target_pairs={{0,4},{4,8},{8,12},{1,5},{5,9},{9,13},{2,6},{6,10},{10,14},{3,7},{... | collective-permute-start | bytes 24584 | tf_op jit(solution)/shard_map/ppermute | solution.py:22
  36.2 1.3 collective-permute-start.4
  37.6 24.0 %all_gather.20 = bf16[2048,128]{1,0:T(8,128)(2,1)S(1)} all-gather(bf16[512,128]{1,0:T(8,128)(2,1)S(1)} %copy-done.1), channel_id=1, replica_groups=mesh['grp'=2,'sp'=4,'tp'=4] {'sp'}, dimensions={0}, use_global_device_ids=true | all-gather | bytes 655360 | tf_op jit(solution)/shard_map/all_gather | solution.py:70
  62.7 14.9 %all_gather.21 = bf16[640,128]{1,0:T(8,128)(2,1)S(1)} all-gather(bf16[160,128]{1,0:T(8,128)(2,1)S(1)} %convolution_convert_fusion.1), channel_id=1, replica_groups=mesh['grp'=2,'sp'=4,'tp'=4] {'sp'}, dimensions={0}, use_global_device_ids=true | all-gather | bytes 204800 | tf_op jit(solution)/shard_map/all_gather | solution.py:107
  77.6 1.0 collective-permute-start.2
  78.6 4.8 %collective-permute-done.2 = bf16[160,128]{1,0:T(8,128)(2,1)S(1)} collective-permute-done((bf16[160,128]{1,0:T(8,128)(2,1)S(1)}, bf16[160,128]{1,0:T(8,128)(2,1)S(1)}, u32[]{:S(2)}, u32[]{:S(2)}) %collective-permute-start.2) | collective-permute-done | bytes 40992 | tf_op jit(solution)/shard_map/ppermute | solution.py:103
  84.0 2.1 %convolution_convert_fusion = bf16[160,512]{1,0:T(8,128)(2,1)S(1)} fusion(bf16[160,2048]{1,0:T(8,128)(2,1)S(1)} %fusion.17, bf16[2048,512]{1,0:T(8,128)(2,1)} %all-gather.4.cloned.1.call-done), kind=kOutput, calls=%fused_computation.29 | convolution fusion | flops 335626240 | bytes 2916352 | tf_op jit(solution)/shard_map/dot_general | solution.py:34
  86.3 8.5 %while.15 = (s32[]{:T(128)}, f32[1,4,2,160]{3,1,2,0:T(4,128)S(1)}, f32[1,4,2,160]{3,1,2,0:T(4,128)S(1)}, f32[1,4,2,160,128]{4,3,2,1,0:T(8,128)S(1)}, bf16[5,128,...) while((s32[]{:T(128)}, f32[1,4,2,160]{3,1,2,0:T(4,128)S(1)}, ...), condition=%wide.region_4.5_spmd.clone, body=%wide.region_1.4_spmd.clone.sunk | while | flops 64232960 | bytes 3694705 | solution.py:112
  86.3 0.6 fusion.78
  88.0 0.6 fusion.78
  89.7 0.6 fusion.78
  91.4 0.6 fusion.78
  93.1 0.6 fusion.78
  95.7 24.1 %all-gather.6.cloned.1.call-done = bf16[512,2048]{1,0:T(8,128)(2,1)} async-done(((bf16[512,512]{1,0:T(8,128)(2,1)}), bf16[512,2048]{1,0:T(8,128)(2,1)}) %all-gather.6.cloned.1.call-update) | async-done | bytes 2097168 | tf_op jit(solution)/shard_map/all_gather | solution.py:147
  119.8 2.1 %fusion.21 = f32[160,2048]{1,0:T(8,128)S(1)} fusion(bf16[512,2048]{1,0:T(8,128)(2,1)} %all-gather.6.cloned.1.call-done, bf16[20,8,4,128]{3,2,1,0:T(4,128)(2,1)S(1)} %bitcast.102), kind=kOutput, calls=%fused_computation.42 | convolution fusion | flops 335544320 | bytes 3571712 | tf_op jit(solution)/shard_map/dot_general | solution.py:152
  121.9 44.0 %all-gather.8.cloned.1.call-done = bf16[512,2048]{1,0:T(8,128)(2,1)} async-done(((bf16[512,512]{1,0:T(8,128)(2,1)}), bf16[512,2048]{1,0:T(8,128)(2,1)}) %all-gather.8.cloned.1.call-update) | async-done | bytes 2097168 | tf_op jit(solution)/shard_map/all_gather | solution.py:148
  165.9 4.3 %fusion.14 = bf16[160,2048]{1,0:T(8,128)(2,1)} fusion(f32[160,2048]{1,0:T(8,128)S(1)} %fusion.21, bf16[512,2048]{1,0:T(8,128)(2,1)} %all-gather.8.cloned.1.call-done, bf16[160,512]{1,0:T(8,128)(2,1)S(1)} %constant_dynamic-slice_fusion.1, f32[160]{0:T(256)S(1)} %subtract_convert_fusion.2, bf16[176,512]{1,0:T(8,128)(2,1)S(1)} %pad_maximum_fusion, ...), kind=kOutput, calls=%fused_computation.23 | convolution fusion | flops 340377600 | bytes 6849616 | tf_op jit(solution)/shard_map/dot_general | solution.py:153
  170.3 0.6 add_bitcast_fusion
  170.9 20.8 %reduce-scatter.2.cloned.1.call-done = bf16[40,2048]{1,0:T(8,128)(2,1)} async-done(((bf16[160,2048]{1,0:T(8,128)(2,1)}), bf16[40,2048]{1,0:T(8,128)(2,1)}) %reduce-scatter.2.cloned.1.call-update) | async-done | bytes 163856 | tf_op jit(solution)/shard_map/reduce_scatter | solution.py:150
  (82 shorter events, 8.2 us)
Async XLA Ops:
  7.2 24.9 %copy-start = (bf16[160,2048]{1,0:T(8,128)(2,1)S(1)}, bf16[160,2048]{1,0:T(8,128)(2,1)}, u32[]{:S(2)}) copy-start(bf16[160,2048]{1,0:T(8,128)(2,1)} %param.11) | copy-start | bytes 1966084
  7.2 24.9 %copy-start.2 = (f32[2048]{0:T(1024)S(1)}, f32[2048]{0:T(1024)}, u32[]{:S(2)}) copy-start(f32[2048]{0:T(1024)} %param.12) | copy-start | bytes 24580
  7.2 76.8 %all-gather.4.cloned.1.call-start = ((), (), s32[]{:S(2)}) async-start(), calls=%async_computation.1 | async-start | bytes 2621440 | tf_op jit(solution)/shard_map/all_gather | solution.py:68
  7.9 111.9 %all-gather.6.cloned.1.call-start = ((), (), s32[]{:S(2)}) async-start(), calls=%async_computation.2 | async-start | bytes 2621440 | tf_op jit(solution)/shard_map/all_gather | solution.py:147
  8.7 157.2 %all-gather.8.cloned.1.call-start = ((), (), s32[]{:S(2)}) async-start(), calls=%async_computation.3 | async-start | bytes 2621440 | tf_op jit(solution)/shard_map/all_gather | solution.py:148
  10.0 27.6 %copy-start.1 = (bf16[512,128]{1,0:T(8,128)(2,1)S(1)}, bf16[512,128]{1,0:T(8,128)(2,1)}, u32[]{:S(2)}) copy-start(bf16[512,128]{1,0:T(8,128)(2,1)} %param.15) | copy-start | bytes 393220
  32.6 29.5 %collective-permute-start = (bf16[160,128]{1,0:T(8,128)(2,1)S(1)}, bf16[160,128]{1,0:T(8,128)(2,1)S(1)}, u32[]{:S(2)}, u32[]{:S(2)}) collective-permute-start(bf16[160,128]{1,0:T(8,128)(2,1)S(1)} %convolution_convert_fusion.2), channel_id=1, source_target_pairs={{0,4},{4,8},{8,12},{12,0},{1,5},{5,9},{9,13},{13,1},{2,6},{6,10},{... | collective-permute-start | bytes 122888 | tf_op jit(solution)/shard_map/ppermute | solution.py:103
  33.6 45.0 %collective-permute-start.3 = (bf16[8,512]{1,0:T(8,128)(2,1)S(1)}, bf16[8,512]{1,0:T(8,128)(2,1)S(1)}, u32[]{:S(2)}, u32[]{:S(2)}) collective-permute-start(bf16[8,512]{1,0:T(8,128)(2,1)S(1)} %get-tuple-element.102), channel_id=1, source_target_pairs={{0,4},{4,8},{8,12},{1,5},{5,9},{9,13},{2,6},{6,10},{10,14},{3,7},{... | collective-permute-start | bytes 24584 | tf_op jit(solution)/shard_map/ppermute | solution.py:22
  36.2 42.4 %collective-permute-start.4 = (bf16[8,512]{1,0:T(8,128)(2,1)S(1)}, bf16[8,512]{1,0:T(8,128)(2,1)S(1)}, u32[]{:S(2)}, u32[]{:S(2)}) collective-permute-start(bf16[8,512]{1,0:T(8,128)(2,1)S(1)} %get-tuple-element.103), channel_id=1, source_target_pairs={{4,0},{8,4},{12,8},{5,1},{9,5},{13,9},{6,2},{10,6},{14,10},{7,3},{... | collective-permute-start | bytes 24584 | tf_op jit(solution)/shard_map/ppermute | solution.py:24
  37.5 154.1 %reduce-scatter.2.cloned.1.call-start = ((), (), s32[]{:S(2)}) async-start(), calls=%async_computation.4 | async-start | bytes 819200 | tf_op jit(solution)/shard_map/reduce_scatter | solution.py:150
  62.1 15.5 %collective-permute-start.1 = (bf16[160,128]{1,0:T(8,128)(2,1)S(1)}, bf16[160,128]{1,0:T(8,128)(2,1)S(1)}, u32[]{:S(2)}, u32[]{:S(2)}) collective-permute-start(bf16[160,128]{1,0:T(8,128)(2,1)S(1)} %collective-permute-done), channel_id=1, source_target_pairs={{0,4},{4,8},{8,12},{12,0},{1,5},{5,9},{9,13},{13,1},{2,6},{6,10},{... | collective-permute-start | bytes 122888 | tf_op jit(solution)/shard_map/ppermute | solution.py:103
  77.6 5.8 %collective-permute-start.2 = (bf16[160,128]{1,0:T(8,128)(2,1)S(1)}, bf16[160,128]{1,0:T(8,128)(2,1)S(1)}, u32[]{:S(2)}, u32[]{:S(2)}) collective-permute-start(bf16[160,128]{1,0:T(8,128)(2,1)S(1)} %collective-permute-done.1), channel_id=1, source_target_pairs={{0,4},{4,8},{8,12},{12,0},{1,5},{5,9},{9,13},{13,1},{2,6},{6,10},{... | collective-permute-start | bytes 122888 | tf_op jit(solution)/shard_map/ppermute | solution.py:103
  86.3 8.8 %copy-start.4 = (f32[4]{0:T(128)S(1)}, f32[4]{0:T(128)}, u32[]{:S(2)}) copy-start(f32[4]{0:T(128)} %param.16) | copy-start | bytes 52
  86.3 9.1 %copy-start.3 = (f32[4,128]{1,0:T(4,128)S(1)}, f32[4,128]{1,0:T(4,128)}, u32[]{:S(2)}) copy-start(f32[4,128]{1,0:T(4,128)} %param.17) | copy-start | bytes 6148
Sparse Core Ops, SparseCore 0:
  9.6 63.5 all-gather.3
  74.7 45.0 all-gather.5
  121.4 44.5 all-gather.7
  170.4 21.2 reduce-scatter.1
